TPU v7x, 256 devices: a whole 4x4x8 slice. The times are simulated.
256 devices in a mesh: sp: 64 (over z, x, core), tp: 4 (over y).
Axes of the slice: x: 4, y: 4, z: 8, core: 2. Of those that a mesh axis runs over, the one named last changes fastest.
Arguments:
- queries: bfloat16 [40960, 1024], P('sp', 'tp'), may hold values from -160 to 160
- keys: bfloat16 [40960, 256], P('sp', 'tp'), may hold values from -24 to 24
- values: bfloat16 [40960, 256], P('sp', 'tp'), may hold values from -6 to 6
- documents: int32 [40960], P('sp'), may hold values from 0 to 15, never falling along the last dimension, each value on 1 to 5120 neighbouring positions
- sinks: float32 [16], P('tp'), may hold values from -1 to 4
- out_weight: bfloat16 [1024, 2048], replicated, may hold values from -0.1875 to 0.1875
- residual: bfloat16 [40960, 2048], P(('sp', 'tp')), may hold values from -3 to 3
- norm_gain: float32 [2048], replicated, may hold values from 0.1 to 1.9
- up_weight: bfloat16 [2048, 8192], P('sp', 'tp'), may hold values from -0.125 to 0.125
- down_weight: bfloat16 [8192, 2048], P('tp', 'sp'), may hold values from -0.0625 to 0.0625
Outputs:
- layer_out: bfloat16 [40960, 2048], P(('sp', 'tp'))
Inputs may be any that keep to these rules, and one draw needn't show every extreme that they name: `documents`: document numbers never fall along the positions; each document holds at most 5120 positions.
All inputs are finite; a program needn't handle non-finite values.
Results may differ from a plain program's by a relative error of at most 0.0095.
Values may be sent and summed in bfloat16 or wider, within the bound.
A program may use at most 64 MiB of HBM per device.

v0:
```python
import jax
import jax.numpy as jnp
from jax import lax
from jax.sharding import PartitionSpec as P

HEAD_SIZE = 64
WINDOW_REACH = 128


masked_score = -1e30
epsilon = 1e-06


def passed_along(shard, axis, by):
    peers = lax.axis_size(axis)
    pairs = [(i, i + by) for i in range(peers) if 0 <= i + by < peers]
    return lax.ppermute(shard, axis, pairs)


def gather_turned(arrays, axis, dims):
    turned = [jnp.moveaxis(a, dim, 0) for a, dim in zip(arrays, dims)]
    widths = [t[0].size for t in turned]
    both = jnp.concatenate([t.reshape(-1, w) for t, w in zip(turned, widths)], axis=1)
    whole = lax.all_gather(both, axis, axis=0, tiled=True)
    pieces = jnp.split(whole, [sum(widths[:k]) for k in range(1, len(widths))], axis=1)
    return tuple(
        (
            jnp.moveaxis(b.reshape(-1, *t.shape[1:]), 0, dim)
            for b, t, dim in zip(pieces, turned, dims)
        )
    )


def from_everyone(shard, axis):
    peers = lax.axis_size(axis)
    return lax.all_to_all(
        jnp.broadcast_to(shard[None], (peers, *shard.shape)), axis, 0, 0, tiled=True
    )


def in_order(pieces, dim):
    dims = list(pieces.shape[1:])
    dims[dim] *= pieces.shape[0]
    return jnp.moveaxis(pieces, 0, dim).reshape(dims)


def gather_directly(shard, axis, dim):
    pieces = from_everyone(shard, axis)
    return in_order(pieces, dim)


def rounded(value):
    return lax.optimization_barrier(value.astype(jnp.bfloat16))


def squared_relu(before):
    return jnp.square(jax.nn.relu(before)).astype(jnp.bfloat16)


def windowed_attention(queries, keys, values, documents, sinks):
    length = queries.shape[0]
    heads = queries.shape[1] // HEAD_SIZE
    kv_heads = keys.shape[1] // HEAD_SIZE
    query_group = heads // kv_heads
    block_list = length // WINDOW_REACH
    prev_keys, prev_values, prev_docs = passed_along(
        (
            keys[length - WINDOW_REACH :],
            values[length - WINDOW_REACH :],
            documents[length - WINDOW_REACH :],
        ),
        "sp",
        1,
    )
    offset = lax.axis_index("sp") * length
    key_matrix = jnp.concatenate([prev_keys, keys], axis=0).reshape(
        block_list + 1, WINDOW_REACH, kv_heads, HEAD_SIZE
    )
    value_matrix = jnp.concatenate([prev_values, values], axis=0).reshape(
        block_list + 1, WINDOW_REACH, kv_heads, HEAD_SIZE
    )
    key_docs = jnp.concatenate([prev_docs, documents], axis=0).reshape(block_list + 1, WINDOW_REACH)
    key_place = (
        offset - WINDOW_REACH + jnp.arange((block_list + 1) * WINDOW_REACH, dtype=jnp.int32)
    ).reshape(block_list + 1, WINDOW_REACH)
    band_keys = jnp.concatenate([key_matrix[:-1], key_matrix[1:]], axis=1)
    band_values = jnp.concatenate([value_matrix[:-1], value_matrix[1:]], axis=1)
    band_docs = jnp.concatenate([key_docs[:-1], key_docs[1:]], axis=1)
    band_place = jnp.concatenate([key_place[:-1], key_place[1:]], axis=1)
    query_docs = documents.reshape(block_list, WINDOW_REACH)
    grouped_queries = queries.reshape(block_list, WINDOW_REACH, kv_heads, query_group, HEAD_SIZE)
    scores = jnp.einsum(
        "nqhgd,nshd->nhgqs", grouped_queries, band_keys, preferred_element_type=jnp.float32
    ) * HEAD_SIZE ** (-0.5)
    row_index = jnp.arange(WINDOW_REACH, dtype=jnp.int32)[:, None]
    col_index = jnp.arange(2 * WINDOW_REACH, dtype=jnp.int32)[None, :]
    distance = WINDOW_REACH + row_index - col_index
    near = (distance >= 0) & (distance < WINDOW_REACH)
    visible = (
        near[None]
        & (band_docs[:, None, :] == query_docs[:, :, None])
        & (band_place[:, None, :] >= 0)
    )
    visible = visible[:, None, None]
    head_sink_logit = sinks.reshape(kv_heads, query_group)[None, :, :, None]
    scores = jnp.where(visible, scores, masked_score)
    top = jnp.maximum(jnp.max(scores, axis=-1), head_sink_logit)
    exponent = jnp.where(visible, jnp.exp(scores - top[..., None]), 0.0)
    total = jnp.exp(head_sink_logit - top) + jnp.sum(exponent, axis=-1)
    shares = (exponent / total[..., None]).astype(jnp.bfloat16)
    attended = jnp.einsum(
        "nhgqs,nshd->nqhgd", shares, band_values, preferred_element_type=jnp.float32
    )
    return attended.astype(jnp.bfloat16).reshape(length, heads * HEAD_SIZE)


def body(
    queries, keys, values, documents, sinks, out_weight, residual, norm_gain, up_weight, down_weight
):
    up_whole, down_whole = gather_turned((up_weight, down_weight), "sp", (0, 1))
    attended = windowed_attention(queries, keys, values, documents, sinks)
    token_heads = lax.all_to_all(attended, "tp", split_axis=0, concat_axis=1, tiled=True)
    projected = jnp.dot(token_heads, out_weight, preferred_element_type=jnp.float32)
    mixed = rounded(residual.astype(jnp.float32) + rounded(projected).astype(jnp.float32))
    widened = mixed.astype(jnp.float32)
    normed = (
        widened
        * lax.rsqrt(jnp.mean(widened * widened, axis=-1, keepdims=True) + epsilon)
        * norm_gain
    ).astype(jnp.bfloat16)
    hidden = squared_relu(
        jnp.dot(gather_directly(normed, "tp", 0), up_whole, preferred_element_type=jnp.float32)
    )
    branch = lax.psum_scatter(
        jnp.dot(hidden, down_whole, preferred_element_type=jnp.float32).astype(jnp.bfloat16),
        "tp",
        scatter_dimension=0,
        tiled=True,
    ).astype(jnp.float32)
    return (widened + rounded(branch).astype(jnp.float32)).astype(jnp.bfloat16)


def solution(mesh):
    in_specs = (
        P("sp", "tp"),
        P("sp", "tp"),
        P("sp", "tp"),
        P("sp"),
        P("tp"),
        P(),
        P(("sp", "tp"), None),
        P(),
        P("sp", "tp"),
        P("tp", "sp"),
    )
    out_specs = P(("sp", "tp"), None)
    return jax.shard_map(body, mesh=mesh, in_specs=in_specs, out_specs=out_specs, check_vma=False)
```

profile of v0, /device:TPU:1, one launch (start us, length us, event | category | flops | bytes accessed | tf_op | source)
XLA Modules:
  0.0 174.1 jit_solution(4770749541361967209)
XLA Ops:
  6.5 0.0 copy-start.3
  6.5 0.0 copy-start.1
  6.5 0.0 copy-start.2
  6.5 0.0 all-gather.2.cloned.1.call-start
  6.5 1.7 pad_maximum_fusion
  8.3 0.0 all-gather.2.cloned.1.call-update
  8.3 0.0 reduce-scatter.2.cloned.1.call-start
  8.3 0.7 slice.63
  9.0 4.5 %collective-permute-start.1 = (s32[128]{0:T(128)S(1)}, s32[128]{0:T(128)S(1)}, u32[]{:S(2)}, u32[]{:S(2)}) collective-permute-start(s32[128]{0:T(128)S(1)} %slice.63), channel_id=1, source_target_pairs={{0,4},{4,8},{8,12},{12,16},{16,20},{20,24},{24,28},{28,32},{32,36}... | collective-permute-start | bytes 1544 | tf_op jit(solution)/shard_map/ppermute | solution.py:17
  13.5 0.7 slice.69
  14.3 1.9 %collective-permute-start.2 = (bf16[128,64]{0,1:T(8,128)(2,1)S(1)}, bf16[128,64]{0,1:T(8,128)(2,1)S(1)}, u32[]{:S(2)}, u32[]{:S(2)}) collective-permute-start(bf16[128,64]{0,1:T(8,128)(2,1)S(1)} %slice.69), channel_id=1, source_target_pairs={{0,4},{4,8},{8,12},{12,16},{16,20},{20,24},{24,28},{28,32},{32,36}... | collective-permute-start | bytes 49160 | tf_op jit(solution)/shard_map/ppermute | solution.py:17
  16.2 0.7 slice.59
  16.9 3.5 %collective-permute-start = (bf16[128,64]{0,1:T(8,128)(2,1)S(1)}, bf16[128,64]{0,1:T(8,128)(2,1)S(1)}, u32[]{:S(2)}, u32[]{:S(2)}) collective-permute-start(bf16[128,64]{0,1:T(8,128)(2,1)S(1)} %slice.59), channel_id=1, source_target_pairs={{0,4},{4,8},{8,12},{12,16},{16,20},{20,24},{24,28},{28,32},{32,36}... | collective-permute-start | bytes 49160 | tf_op jit(solution)/shard_map/ppermute | solution.py:17
  20.5 1.0 slice.72
  21.5 1.0 slice.62
  22.5 1.3 reshape.148
  23.9 0.0 copy-start.5
  23.9 0.0 collective-permute-done.1
  23.9 0.0 copy-done.3
  23.9 0.5 and_and_fusion
  24.5 0.0 collective-permute-done.2
  24.5 0.0 copy-done.1
  24.5 0.1 slice.71
  24.6 0.0 collective-permute-done
  24.6 0.0 copy-done.2
  24.7 0.1 slice.61
  24.8 0.6 fusion.14
  25.4 0.0 copy-done.5
  25.5 0.1 broadcast_maximum_fusion
  25.5 0.7 fusion.15
  26.2 0.1 exponential_add_fusion
  26.3 0.9 fusion.26
  27.1 1.0 copy.20
  28.2 0.4 all_to_all.17
  28.6 11.3 %all_to_all.24 = bf16[4,160,256]{2,1,0:T(8,128)(2,1)S(1)} all-to-all(bf16[4,160,256]{2,1,0:T(8,128)(2,1)S(1)} %all_to_all.17), channel_id=1, replica_groups=mesh['sp'=64,'tp'=4] {'tp'}, dimensions={0} | all-to-all | bytes 655360 | tf_op jit(solution)/shard_map/all_to_all | solution.py:122
  39.9 0.0 copy-start
  39.9 0.0 copy-start.4
  39.9 3.1 %convolution_convert_fusion = bf16[160,2048]{1,0:T(8,128)(2,1)S(1)} fusion(bf16[160,1024]{1,0:T(8,128)(2,1)S(1)} %bitcast.66, bf16[1024,2048]{1,0:T(8,128)(2,1)} %param.15), kind=kOutput, calls=%fused_computation.10 | convolution fusion | flops 671416320 | bytes 5177344 | tf_op jit(solution)/shard_map/dot_general | solution.py:123
  43.1 0.0 copy-done
  43.1 0.2 add_convert_fusion
  43.3 0.2 fusion.16
  43.5 0.0 copy-done.4
  43.5 0.2 fusion.18
  43.7 0.3 broadcast_in_dim.37
  44.1 34.1 %all_to_all.25 = bf16[4,160,2048]{2,1,0:T(8,128)(2,1)S(1)} all-to-all(bf16[4,160,2048]{2,1,0:T(8,128)(2,1)S(1)} %broadcast_in_dim.37), channel_id=1, replica_groups=mesh['sp'=64,'tp'=4] {'tp'}, dimensions={0} | all-to-all | bytes 5242880 | tf_op jit(solution)/shard_map/all_to_all | solution.py:36
  78.2 35.3 %all-gather.2.cloned.1.call-done = bf16[2048,4096]{1,0:T(8,128)(2,1)} async-done(((bf16[32,4096]{1,0:T(8,128)(2,1)}), bf16[2048,4096]{1,0:T(8,128)(2,1)}) %all-gather.2.cloned.1.call-update) | async-done | bytes 16777232 | tf_op jit(solution)/shard_map/all_gather | solution.py:24
  113.5 18.2 %fusion.8 = bf16[640,2048]{1,0:T(8,128)(2,1)} fusion(bf16[2048,4096]{1,0:T(8,128)(2,1)} %all-gather.2.cloned.1.call-done, bf16[640,2048]{1,0:T(8,128)(2,1)S(1)} %bitcast.65), kind=kOutput, calls=%fused_computation.5 | convolution fusion | flops 10742661120 | bytes 22020096 | tf_op jit(solution)/shard_map/dot_general | solution.py:135
  131.8 0.0 reduce-scatter.2.cloned.1.call-update
  131.8 33.3 %reduce-scatter.2.cloned.1.call-done = bf16[160,2048]{1,0:T(8,128)(2,1)} async-done(((bf16[640,2048]{1,0:T(8,128)(2,1)}), bf16[160,2048]{1,0:T(8,128)(2,1)}) %reduce-scatter.2.cloned.1.call-update) | async-done | bytes 655376 | tf_op jit(solution)/shard_map/reduce_scatter | solution.py:134
  165.1 2.1 %fusion.19 = bf16[160,2048]{1,0:T(8,128)(2,1)} fusion(bf16[160,2048]{1,0:T(8,128)(2,1)S(1)} %add_convert_fusion, bf16[160,2048]{1,0:T(8,128)(2,1)} %reduce-scatter.2.cloned.1.call-done), kind=kLoop, calls=%fused_computation.19 | loop fusion | flops 1310720 | bytes 1966080 | tf_op jit(solution)/shard_map/convert_element_type | solution.py:140
  (16 shorter events, 0.2 us)
Async XLA Ops:
  6.5 17.4 %copy-start.3 = (s32[640]{0:T(1024)S(1)}, s32[640]{0:T(1024)}, u32[]{:S(2)}) copy-start(s32[640]{0:T(1024)} %param.13) | copy-start | bytes 7684
  6.5 17.9 %copy-start.1 = (bf16[640,64]{0,1:T(8,128)(2,1)S(1)}, bf16[640,64]{0,1:T(8,128)(2,1)}, u32[]{:S(2)}) copy-start(bf16[640,64]{0,1:T(8,128)(2,1)} %param.11) | copy-start | bytes 245764
  6.5 18.1 %copy-start.2 = (bf16[640,64]{0,1:T(8,128)(2,1)S(1)}, bf16[640,64]{0,1:T(8,128)(2,1)}, u32[]{:S(2)}) copy-start(bf16[640,64]{0,1:T(8,128)(2,1)} %param.12) | copy-start | bytes 245764
  6.5 107.0 %all-gather.2.cloned.1.call-start = ((), (), s32[]{:S(2)}) async-start(), calls=%async_computation.3 | async-start | bytes 17039360 | tf_op jit(solution)/shard_map/all_gather | solution.py:24
  8.3 156.8 %reduce-scatter.2.cloned.1.call-start = ((), (), s32[]{:S(2)}) async-start(), calls=%async_computation.4 | async-start | bytes 3276800 | tf_op jit(solution)/shard_map/reduce_scatter | solution.py:134
  9.0 14.8 %collective-permute-start.1 = (s32[128]{0:T(128)S(1)}, s32[128]{0:T(128)S(1)}, u32[]{:S(2)}, u32[]{:S(2)}) collective-permute-start(s32[128]{0:T(128)S(1)} %slice.63), channel_id=1, source_target_pairs={{0,4},{4,8},{8,12},{12,16},{16,20},{20,24},{24,28},{28,32},{32,36}... | collective-permute-start | bytes 1544 | tf_op jit(solution)/shard_map/ppermute | solution.py:17
  14.3 10.2 %collective-permute-start.2 = (bf16[128,64]{0,1:T(8,128)(2,1)S(1)}, bf16[128,64]{0,1:T(8,128)(2,1)S(1)}, u32[]{:S(2)}, u32[]{:S(2)}) collective-permute-start(bf16[128,64]{0,1:T(8,128)(2,1)S(1)} %slice.69), channel_id=1, source_target_pairs={{0,4},{4,8},{8,12},{12,16},{16,20},{20,24},{24,28},{28,32},{32,36}... | collective-permute-start | bytes 49160 | tf_op jit(solution)/shard_map/ppermute | solution.py:17
  16.9 7.7 %collective-permute-start = (bf16[128,64]{0,1:T(8,128)(2,1)S(1)}, bf16[128,64]{0,1:T(8,128)(2,1)S(1)}, u32[]{:S(2)}, u32[]{:S(2)}) collective-permute-start(bf16[128,64]{0,1:T(8,128)(2,1)S(1)} %slice.59), channel_id=1, source_target_pairs={{0,4},{4,8},{8,12},{12,16},{16,20},{20,24},{24,28},{28,32},{32,36}... | collective-permute-start | bytes 49160 | tf_op jit(solution)/shard_map/ppermute | solution.py:17
  23.9 1.6 copy-start.5
  39.9 3.2 %copy-start = (bf16[160,2048]{1,0:T(8,128)(2,1)S(1)}, bf16[160,2048]{1,0:T(8,128)(2,1)}, u32[]{:S(2)}) copy-start(bf16[160,2048]{1,0:T(8,128)(2,1)} %param.16) | copy-start | bytes 1966084
  39.9 3.6 %copy-start.4 = (f32[2048]{0:T(1024)S(1)}, f32[2048]{0:T(1024)}, u32[]{:S(2)}) copy-start(f32[2048]{0:T(1024)} %param.17) | copy-start | bytes 24580
Sparse Core Ops, SparseCore 0:
  10.1 103.3 all-gather.1
  131.9 33.1 reduce-scatter.1
where the time goes:
time: 175 us; the launch traced here: 174 us
  waiting for transfers between devices  68.6 us (39%)
  blocking collectives  45.4 us (26%)
  matrix products  22.9 us (13%)
  between operations  13.7 us (8%)
  starting transfers between devices  9.93 us (6%)
  local copies, waits for them, and re-layouts  7.54 us (4%)
  other arithmetic  5.93 us (3%)
    all_gather x1, waiting for transfers between devices, gather_turned(): whole = lax.all_gather(both, axis, axis=0, tiled=True)  35.3 us
    all_to_all x1, blocking collectives, from_everyone(): lax.all_to_all(jnp.broadcast_to(shard[None], (peers, *shard.shape)), axis...  34.1 us
    reduce_scatter x1, waiting for transfers between devices, body(): lax.psum_scatter(jnp.dot(hidden, down_whole, preferred_element_type=jnp.f...  33.3 us
    dot_general x1, matrix products, body(): jnp.dot(hidden, down_whole, preferred_element_type=jnp.float32)  18.2 us
    all_to_all x1, blocking collectives, body(): lax.all_to_all(attended, 'tp', split_axis=0, concat_axis=1, tiled=True)  11.3 us
    ppermute x3, starting transfers between devices, passed_along(): return lax.ppermute(shard, axis, pairs)  9.88 us
  transfers between devices with their start and end apart: 5, of which 2 were waited for; matrix products, arithmetic and copies ran while one was open for 8% of the time, Pallas kernels for 0%

commit v1 on v0

v1 whole, which is shorter than its diff:
```python
import functools
import heapq

import jax
import jax.numpy as jnp
from jax import lax
from jax.experimental import pallas as pl
from jax.experimental.pallas import tpu as pltpu
from jax.sharding import PartitionSpec as P

MESH = pl.DeviceIdType.MESH
NZ, NX, NY = 8, 4, 4
HEAD = 64
REACH = 128
TOK = 640
OWN = 160
HALF = 80
D = 2048
SHARD = 32
masked_score = -1e30
epsilon = 1e-06

STREAMS = ((0, "z", 0, D), (1, "x", 0, D))
RATE = 46.6e3
LATENCY = 1.8
DZ_ORDER = (0, 1, -1, 2, -2, 3, -3, 4)


def onward(item):
    s, dz, dx, part = item
    mode = STREAMS[s][1]
    out = []

    def along_z():
        if dz == 0:
            out.append(("z", 1, (s, 1, dx, None)))
            out.append(("z", -1, (s, -1, dx, None)))
        elif dz in (1, 2):
            out.append(("z", 1, (s, dz + 1, dx, None)))
        elif dz in (-1, -2):
            out.append(("z", -1, (s, dz - 1, dx, None)))
        elif dz == 3:
            out.append(("z", 1, (s, 4, dx, 0)))
        elif dz == -3:
            out.append(("z", -1, (s, 4, dx, 1)))

    def along_x():
        if dx == 0:
            out.append(("x", 1, (s, dz, 1, part)))
            out.append(("x", -1, (s, dz, -1, part)))
        elif dx == 1:
            if dz == 0:
                out.append(("x", 1, (s, dz, 2, 0)))
            elif dz in (1, -2, 3) or (dz == 4 and part == 0):
                out.append(("x", 1, (s, dz, 2, part)))
        elif dx == -1:
            if dz == 0:
                out.append(("x", -1, (s, dz, 2, 1)))
            elif dz in (-1, 2, -3) or (dz == 4 and part == 1):
                out.append(("x", -1, (s, dz, 2, part)))

    if mode == "z":
        if dx == 0:
            along_z()
        along_x()
    else:
        if dz == 0:
            along_x()
        if part is None or dz != 0:
            if part is None:
                along_z()
        elif part == 1:
            along_z()
    return out


def plan():
    free = {}
    heap = []

    def put(now, item):
        for axis, way, there in onward(item):
            size = SHARD * STREAMS[there[0]][3] * 2
            if there[3] is not None:
                size //= 2
            begin = max(now, free.get((axis, way), 0.0))
            end = begin + size / RATE
            free[(axis, way)] = end
            heapq.heappush(heap, (end + LATENCY, str(there), there))

    for s in range(len(STREAMS)):
        put(0.0, (s, 0, 0, None))
    order = []
    while heap:
        now, _, item = heapq.heappop(heap)
        order.append((now, item))
        put(now, item)
    return order


PLAN = plan()
SLOT = {item: k for k, (_, item) in enumerate(PLAN)}


def kernel(
    q_ref, k_ref, v_ref, docs_ref, sink_ref, w_hbm, res_hbm, gain_ref, up_ref, down_ref,
    out_ref,
    up_all, down_all, w_ref, res_ref, k_band, v_band, k_prev, v_prev, docs_prev, docs_band,
    attended, heads, mixed, normed, hidden, parts, first_a, first_b, last_a, last_b,
    arrive, send_sems, twin_sem, twin_arrive, load_sem, halo_sem, halo_send,
    swap_sem, swap_send, row_sem, row_send, sum_sem, sum_send, end_sem,
):
    sp = lax.axis_index("sp")
    y = lax.axis_index("tp")
    c = lax.rem(sp, 2)
    x = lax.rem(sp // 2, NX)
    z = sp // (2 * NX)

    def place(zz, xx, cc):
        return (zz * NX + xx) * 2 + cc

    def near(axis, way):
        if axis == "z":
            return {"sp": place(lax.rem(z + way + NZ, NZ), x, c), "tp": y}
        return {"sp": place(z, lax.rem(x + way + NX, NX), c), "tp": y}

    twin = {"sp": place(z, x, 1 - c), "tp": y}

    def column(by):
        return {"sp": sp, "tp": lax.rem(y + by + NY, NY)}

    def line(by):
        return {"sp": lax.rem(sp + by + 2 * NX * NZ, 2 * NX * NZ), "tp": y}

    w_load = pltpu.make_async_copy(w_hbm, w_ref, load_sem.at[0])
    res_load = pltpu.make_async_copy(res_hbm, res_ref, load_sem.at[1])
    w_load.start()
    res_load.start()

    barrier = pltpu.get_barrier_semaphore()
    greeted = [near("z", 1), near("z", -1), near("x", 1), near("x", -1), twin,
               column(1), column(2), column(3), line(1), line(-1)]
    for device in greeted:
        pl.semaphore_signal(barrier, inc=1, device_id=device, device_id_type=MESH)
    pl.semaphore_wait(barrier, len(greeted))

    def remote(src, dst, send, recv, device):
        return pltpu.make_async_remote_copy(
            src_ref=src, dst_ref=dst, send_sem=send, recv_sem=recv, device_id=device, device_id_type=MESH
        )

    whole = (up_all, down_all)
    shards = (up_ref, down_ref)

    def view(item):
        s, dz, dx, part = item
        b, _, first, count = STREAMS[s]
        zz = lax.rem(z - dz + 2 * NZ, NZ)
        xx = lax.rem(x - dx + 2 * NX, NX)
        row = place(zz, xx, c) * SHARD
        rows = SHARD
        if part is not None:
            rows = SHARD // 2
            row = row + part * rows
        return whole[b].at[pl.ds(pl.multiple_of(row, 16), rows), pl.ds(first, count)]

    def own_view(s, part):
        b, _, first, count = STREAMS[s]
        if part is None:
            return shards[b].at[:, pl.ds(first, count)]
        return shards[b].at[pl.ds(part * (SHARD // 2), SHARD // 2), pl.ds(first, count)]

    def pass_on(item):
        s, dz, dx, part = item
        b = STREAMS[s][0]
        own = dz == 0 and dx == 0
        for axis, way, there in onward(item):
            here = (s, dz, dx, there[3])
            src = own_view(s, there[3]) if own else view(here)
            remote(src, view(here), send_sems.at[b], arrive.at[SLOT[there]], near(axis, way)).start()
        src = own_view(s, part) if own else view(item)
        remote(src, view(item), twin_sem.at[b], twin_arrive.at[b, DZ_ORDER.index(dz)], twin).start()

    def take(item):
        ref = view(item)
        remote(ref, ref, send_sems.at[0], arrive.at[SLOT[item]], twin).wait_recv()
        pass_on(item)

    queue = list(PLAN)

    def serve(until):
        while queue and queue[0][0] <= until:
            take(queue.pop(0)[1])

    def serve_for(b, dz):
        def missing():
            return any(STREAMS[i[0]][0] == b and i[1] == dz for _, i in queue)
        while missing():
            take(queue.pop(0)[1])

    def twin_wait(b, dz):
        ref = whole[b].at[pl.ds(0, NX * SHARD), :]
        remote(ref, ref, twin_sem.at[b], twin_arrive.at[b, DZ_ORDER.index(dz)], twin).wait_recv()

    for s in range(len(STREAMS)):
        pass_on((s, 0, 0, None))

    last = pl.ds(TOK - REACH, REACH)
    halo = [
        remote(k_ref.at[:, last], k_prev, halo_send.at[0], halo_sem.at[0], line(1)),
        remote(v_ref.at[:, last], v_prev, halo_send.at[1], halo_sem.at[1], line(1)),
        remote(docs_ref.at[:, last], docs_prev, halo_send.at[2], halo_sem.at[2], line(1)),
    ]
    for copy in halo:
        copy.start()

    own_row = pl.multiple_of(place(z, x, c) * SHARD, SHARD)
    up_all[pl.ds(own_row, SHARD), :] = up_ref[...]
    down_all[pl.ds(own_row, SHARD), :] = down_ref[...]

    k_band[:, REACH:] = k_ref[...]
    v_band[:, REACH:] = v_ref[...]
    docs_band[:, REACH:] = docs_ref[...].astype(jnp.float32)
    ahead = (
        REACH
        + lax.broadcasted_iota(jnp.int32, (REACH, 2 * REACH), 0)
        - lax.broadcasted_iota(jnp.int32, (REACH, 2 * REACH), 1)
    )
    in_reach = (ahead >= 0) & (ahead < REACH)

    def attend(block):
        rows = pl.ds(block * REACH, REACH)
        band = pl.ds(block * REACH, 2 * REACH)
        keys = k_band[:, band]
        values = v_band[:, band]
        own_docs = docs_band[:, pl.ds((block + 1) * REACH, REACH)]
        own_docs = jnp.transpose(jnp.broadcast_to(own_docs, (REACH, REACH)))
        own_docs = jnp.concatenate([own_docs, own_docs], axis=1)
        visible = in_reach & (own_docs == docs_band[:, band])
        outs = []
        for h in range(4):
            scores = jnp.dot(
                q_ref[rows, pl.ds(h * HEAD, HEAD)], keys, preferred_element_type=jnp.float32
            ) * HEAD ** (-0.5)
            scores = jnp.where(visible, scores, masked_score)
            sink = sink_ref[h]
            top = jnp.maximum(jnp.max(scores, axis=-1, keepdims=True), sink)
            exponent = jnp.where(visible, jnp.exp(scores - top), 0.0)
            total = jnp.exp(sink - top) + jnp.sum(exponent, axis=-1, keepdims=True)
            shares = (exponent / total).astype(jnp.bfloat16)
            outs.append(
                lax.dot_general(
                    shares, values, (((1,), (1,)), ((), ())), preferred_element_type=jnp.float32
                )
            )
        attended[rows, :] = jnp.concatenate(outs, axis=1).astype(jnp.bfloat16)

    attend(1)
    attend(2)
    serve(4.6)
    attend(3)
    attend(4)
    serve(5.6)
    for copy in halo:
        copy.wait_recv()
    k_band[:, :REACH] = k_prev[...]
    v_band[:, :REACH] = v_prev[...]
    docs_band[:, :REACH] = jnp.where(sp == 0, -1.0, docs_prev[...].astype(jnp.float32))
    attend(0)

    def owner_rows(of, part=None):
        if part is None:
            return pl.ds(pl.multiple_of(of * OWN, 16), OWN)
        return pl.ds(pl.multiple_of(of * OWN + part * HALF, 16), HALF)

    def lanes(of):
        return pl.ds(pl.multiple_of(of * 256, 256), 256)

    swaps = []
    for by in (1, 3, 2):
        swaps.append(remote(
            attended.at[owner_rows(lax.rem(y + by, NY)), :], heads.at[:, lanes(y)],
            swap_send.at[by - 1], swap_sem.at[by - 1], column(by),
        ))
        swaps[-1].start()
    heads[:, lanes(y)] = attended[owner_rows(y), :]
    serve(9.0)
    w_load.wait()
    res_load.wait()
    for by, copy in zip((1, 3, 2), swaps):
        slot = heads.at[:, lanes(lax.rem(y - by + NY, NY))]
        remote(slot, slot, swap_send.at[by - 1], swap_sem.at[by - 1], column(by)).wait_recv()

    def project(n, carry):
        cols = pl.ds(pl.multiple_of(n * 512, 512), 512)
        product = jnp.dot(heads[...], w_ref[:, cols], preferred_element_type=jnp.float32)
        product = product.astype(jnp.bfloat16).astype(jnp.float32)
        mixed[:, cols] = (res_ref[:, cols].astype(jnp.float32) + product).astype(jnp.bfloat16)
        return carry

    lax.fori_loop(0, 4, project, 0)

    def norm(i, carry):
        widened = mixed[pl.ds(pl.multiple_of(i * 32, 32), 32), :].astype(jnp.float32)
        scale = lax.rsqrt(jnp.mean(widened * widened, axis=-1, keepdims=True) + epsilon)
        normed[pl.ds(pl.multiple_of(y * OWN + i * 32, 32), 32), :] = (
            widened * scale * gain_ref[...]
        ).astype(jnp.bfloat16)
        return carry

    lax.fori_loop(0, 5, norm, 0)

    def row_copy(of, part, by, slot):
        ref = normed.at[owner_rows(of, part), :]
        return remote(ref, ref, row_send.at[0], row_sem.at[slot], column(by))

    row_copy(y, 0, 1, 0).start()
    row_copy(y, 1, -1, 3).start()
    row_copy(y, 1, 1, 1).start()
    row_copy(y, 0, -1, 2).start()
    before, after, across = lax.rem(y + 3, NY), lax.rem(y + 1, NY), lax.rem(y + 2, NY)
    serve(21.0)
    row_copy(before, 0, 1, 0).wait_recv()
    row_copy(before, 0, 1, 4).start()
    row_copy(after, 1, -1, 3).wait_recv()
    row_copy(after, 1, -1, 5).start()
    serve(29.0)
    row_copy(before, 1, 1, 1).wait_recv()
    row_copy(after, 0, -1, 2).wait_recv()
    serve(35.0)
    row_copy(across, 0, 1, 4).wait_recv()
    row_copy(across, 1, -1, 5).wait_recv()
    for dz in DZ_ORDER:
        serve_for(0, dz)
    for dz in DZ_ORDER:
        twin_wait(0, dz)

    def expand(n, carry):
        cols = pl.ds(pl.multiple_of(n * 512, 512), 512)
        before_act = jnp.dot(normed[...], up_all[:, cols], preferred_element_type=jnp.float32)
        hidden[:, cols] = jnp.square(jnp.maximum(before_act, 0.0)).astype(jnp.bfloat16)
        return carry

    for half in range(2):
        lax.fori_loop(2 * half, 2 * half + 2, expand, 0)
        serve(44.0)

    def add_and_send(i):
        for way, (first, last_buf, part) in enumerate(((first_a, last_a, 0), (first_b, last_b, 1))):
            by = 1 if way == 0 else -1
            to = lax.rem(y + by + NY, NY)
            ref = first.at[i]
            remote(ref, ref, sum_send.at[0], sum_sem.at[i, way], column(by)).wait_recv()
            rows = owner_rows(to, part)
            parts[i, rows, :] = (
                parts[i, rows, :].astype(jnp.float32) + first[i].astype(jnp.float32)
            ).astype(jnp.bfloat16)
            remote(parts.at[i, owner_rows(to), :], last_buf.at[i], sum_send.at[0], end_sem.at[i, way],
                   column(by)).start()

    for i, dz in enumerate(DZ_ORDER):
        serve_for(1, dz)
        twin_wait(1, dz)
        zz = lax.rem(z - dz + 2 * NZ, NZ)
        parts[i] = lax.dot_general(
            hidden[...], down_all[pl.ds(pl.multiple_of(zz * 256, 256), 256), :],
            (((1,), (1,)), ((), ())), preferred_element_type=jnp.float32,
        ).astype(jnp.bfloat16)
        remote(parts.at[i, owner_rows(across, 0), :], first_a.at[i], sum_send.at[0], sum_sem.at[i, 0],
               column(1)).start()
        remote(parts.at[i, owner_rows(across, 1), :], first_b.at[i], sum_send.at[0], sum_sem.at[i, 1],
               column(-1)).start()
        if i >= 1:
            add_and_send(i - 1)
    add_and_send(len(DZ_ORDER) - 1)
    for i, dz in enumerate(DZ_ORDER):
        zz = lax.rem(z - dz + 2 * NZ, NZ)
        for way, last_buf in enumerate((last_a, last_b)):
            ref = last_buf.at[i]
            remote(ref, ref, sum_send.at[0], end_sem.at[i, way], column(1)).wait_recv()
        branch = (
            parts[i, owner_rows(y), :].astype(jnp.float32)
            + last_a[i].astype(jnp.float32)
            + last_b[i].astype(jnp.float32)
        )
        branch = branch.astype(jnp.bfloat16).astype(jnp.float32)
        out_ref[:, lanes(zz)] = (mixed[:, lanes(zz)].astype(jnp.float32) + branch).astype(jnp.bfloat16)

    for b in range(2):
        ref = whole[b].at[pl.ds(0, 31 * SHARD), :]
        remote(ref, ref, send_sems.at[b], arrive.at[0], twin).wait_send()
        ref = whole[b].at[pl.ds(0, 32 * SHARD), :]
        remote(ref, ref, twin_sem.at[b], arrive.at[0], twin).wait_send()
    for copy in halo:
        copy.wait_send()
    for copy in swaps:
        copy.wait_send()
    ref = normed.at[pl.ds(0, 3 * OWN), :]
    remote(ref, ref, row_send.at[0], arrive.at[0], twin).wait_send()
    ref = parts.at[:, pl.ds(0, 3 * OWN), :]
    remote(ref, ref, sum_send.at[0], arrive.at[0], twin).wait_send()


def body(
    queries, keys, values, documents, sinks, out_weight, residual, norm_gain, up_weight, down_weight
):
    vmem = pl.BlockSpec(memory_space=pltpu.VMEM)
    anywhere = pl.BlockSpec(memory_space=pl.ANY)
    bf16 = jnp.bfloat16
    dma = pltpu.SemaphoreType.DMA
    blocks = len(DZ_ORDER)
    return pl.pallas_call(
        kernel,
        out_shape=jax.ShapeDtypeStruct((OWN, D), bf16),
        in_specs=[vmem, vmem, vmem, vmem, pl.BlockSpec(memory_space=pltpu.SMEM), anywhere, anywhere,
                  vmem, vmem, vmem],
        out_specs=vmem,
        scratch_shapes=[
            pltpu.VMEM((D, D), bf16),
            pltpu.VMEM((D, D), bf16),
            pltpu.VMEM((1024, D), bf16),
            pltpu.VMEM((OWN, D), bf16),
            pltpu.VMEM((HEAD, TOK + REACH), bf16),
            pltpu.VMEM((HEAD, TOK + REACH), bf16),
            pltpu.VMEM((HEAD, REACH), bf16),
            pltpu.VMEM((HEAD, REACH), bf16),
            pltpu.VMEM((1, REACH), jnp.int32),
            pltpu.VMEM((1, TOK + REACH), jnp.float32),
            pltpu.VMEM((TOK, 256), bf16),
            pltpu.VMEM((OWN, 1024), bf16),
            pltpu.VMEM((OWN, D), bf16),
            pltpu.VMEM((TOK, D), bf16),
            pltpu.VMEM((TOK, D), bf16),
            pltpu.VMEM((blocks, TOK, 256), bf16),
            pltpu.VMEM((blocks, HALF, 256), bf16),
            pltpu.VMEM((blocks, HALF, 256), bf16),
            pltpu.VMEM((blocks, OWN, 256), bf16),
            pltpu.VMEM((blocks, OWN, 256), bf16),
            dma((len(PLAN),)),
            dma((2,)),
            dma((2,)),
            dma((2, blocks)),
            dma((2,)),
            dma((3,)),
            dma((3,)),
            dma((3,)),
            dma((3,)),
            dma((6,)),
            dma((1,)),
            dma((blocks, 2)),
            dma((1,)),
            dma((blocks, 2)),
        ],
        compiler_params=pltpu.CompilerParams(
            collective_id=0, has_side_effects=True, vmem_limit_bytes=60 * 1024 * 1024
        ),
    )(
        queries, keys.T, values.T, documents.reshape(1, TOK), sinks, out_weight, residual,
        norm_gain.reshape(1, D), up_weight, down_weight.T,
    )


def solution(mesh):
    in_specs = (
        P("sp", "tp"),
        P("sp", "tp"),
        P("sp", "tp"),
        P("sp"),
        P("tp"),
        P(),
        P(("sp", "tp"), None),
        P(),
        P("sp", "tp"),
        P("tp", "sp"),
    )
    out_specs = P(("sp", "tp"), None)
    return jax.shard_map(body, mesh=mesh, in_specs=in_specs, out_specs=out_specs, check_vma=False)
```

time: 175 us -> 95.6 us (0.55)
  Pallas kernels: 0 us -> 92 us
  waiting for transfers between devices: 68.6 us -> 0 us
  blocking collectives: 45.4 us -> 0 us
  matrix products: 22.9 us -> 0 us
  between operations: 13.7 us -> 0.01 us
  starting transfers between devices: 9.93 us -> 0 us
  other arithmetic: 5.93 us -> 0 us
  local copies, waits for them, and re-layouts: 7.54 us -> 3.25 us
    pallas_call x0 -> x1, Pallas kernels: none -> 92 us  [body(): pl.pallas_call(kernel, out_shape=jax.ShapeDtypeStruct((OWN, D), bf16), in...]
    all_to_all x2 -> x0, blocking collectives: 45.4 us -> none  [the longest x1 34.1 us: from_everyone(): lax.all_to_all(jnp.broadcast_to(shard[None], (peers, *shard.shape)), axis...]
    all_gather x1 -> x0, waiting for transfers between devices: 35.3 us -> none  [gather_turned(): whole = lax.all_gather(both, axis, axis=0, tiled=True)]
    reduce_scatter x1 -> x0, waiting for transfers between devices: 33.3 us -> none  [body(): lax.psum_scatter(jnp.dot(hidden, down_whole, preferred_element_type=jnp.f...]
    dot_general x4 -> x0, matrix products: 22.9 us -> none  [the longest x1 18.2 us: body(): jnp.dot(hidden, down_whole, preferred_element_type=jnp.float32)]
    ppermute x3 -> x0, starting transfers between devices: 9.88 us -> none  [passed_along(): return lax.ppermute(shard, axis, pairs)]
    slice x13 -> x0, local copies, waits for them, and re-layouts: 4.42 us -> none  [the longest x4 1.14 us: windowed_attention(): band_keys = jnp.concatenate([key_matrix[:-1], key_matrix[1:]], axis=1)]
    convert_element_type x3 -> x0, other arithmetic: 2.55 us -> none  [the longest x1 2.13 us: body(): return (widened + rounded(branch).astype(jnp.float32)).astype(jnp.bfloat16)]
  transfers between devices with their start and end apart: 5 -> 0, of which waited for: 2 -> 0; matrix products, arithmetic and copies ran while one was open for 8% -> 0% of each run, Pallas kernels for 0% -> 0%
where the time goes in v1:
time: 95.6 us; the launch traced here: 95.2 us
  Pallas kernels  92 us (96%)
  local copies, waits for them, and re-layouts  3.25 us (3%)
    pallas_call x1, Pallas kernels, body(): pl.pallas_call(kernel, out_shape=jax.ShapeDtypeStruct((OWN, D), bf16), in...  92 us
    unnamed x1, local copies, waits for them, and re-layouts  1.98 us

profile of v1, /device:TPU:1, one launch (start us, length us, event | category | flops | bytes accessed | tf_op | source)
XLA Modules:
  0.0 95.2 jit_solution(14585130736883498420)
XLA Ops:
  0.0 1.3 %reshape.6.docs_ref = s32[1,640]{1,0:T(1,128)} reshape(s32[640]{0:T(1024)} %param.13) | data formatting | bytes 5120 | tf_op jit(solution)/shard_map/reshape | solution.py:458
  1.3 92.0 %shard_map.100 = bf16[160,2048]{1,0:T(8,128)(2,1)} custom-call(bf16[640,256]{1,0:T(8,128)(2,1)} %q_ref.1, bf16[64,640]{1,0:T(8,128)(2,1)} %bitcast.5, bf16[64,640]{1,0:T(8,128)(2,1)} %bitcast.6, s32[1,640]{1,0:T(1,128)} %reshape.6.docs_ref, f32[4]{0:T(128)} %sink_ref.1, bf16[1024,2048]{1,0:T(8,128)(2,1)} %w_hbm.1, bf16[160,2048]{1,0:T(8,128)(2,1)} %res_hbm.1, ...), custom_call_target="tpu_custom_call" | custom-call | tf_op jit(solution)/shard_map/pallas_call | solution.py:412
  93.2 2.0 %copy.12 = bf16[160,2048]{1,0:T(8,128)(2,1)} copy(bf16[160,2048]{1,0:T(8,128)(2,1)} %shard_map.100) | data formatting | bytes 1310720

commit v2 on v1

v2 whole, which is shorter than its diff:
```python
import functools
import heapq

import jax
import jax.numpy as jnp
from jax import lax
from jax.experimental import pallas as pl
from jax.experimental.pallas import tpu as pltpu
from jax.sharding import PartitionSpec as P

MESH = pl.DeviceIdType.MESH
NZ, NX, NY = 8, 4, 4
HEAD = 64
REACH = 128
TOK = 640
OWN = 160
HALF = 80
D = 2048
SHARD = 32
masked_score = -1e30
epsilon = 1e-06

CUT = 1280
STREAMS = ((0, "z", 0, CUT), (0, "x", CUT, D - CUT), (1, "z", 0, CUT), (1, "x", CUT, D - CUT))
BEGIN = (0.0, 0.0, 20.0, 20.0)
RATE = 46.6e3
LATENCY = 1.8
TWIN_RATE = 600e3
TWIN_LATENCY = 1.0
ISSUE = 0.015
MARGIN = 0.3
LAG = 3
DZ_ORDER = (0, 1, -1, 2, -2, 3, -3, 4)


def onward(item):
    s, dz, dx, part = item
    mode = STREAMS[s][1]
    out = []

    def along_z():
        if dz == 0:
            out.append(("z", 1, (s, 1, dx, None)))
            out.append(("z", -1, (s, -1, dx, None)))
        elif dz in (1, 2):
            out.append(("z", 1, (s, dz + 1, dx, None)))
        elif dz in (-1, -2):
            out.append(("z", -1, (s, dz - 1, dx, None)))
        elif dz == 3:
            out.append(("z", 1, (s, 4, dx, 0)))
        elif dz == -3:
            out.append(("z", -1, (s, 4, dx, 1)))

    def along_x():
        if dx == 0:
            out.append(("x", 1, (s, dz, 1, part)))
            out.append(("x", -1, (s, dz, -1, part)))
        elif dx == 1:
            if dz == 0:
                out.append(("x", 1, (s, dz, 2, 0)))
            elif dz in (1, -2, 3) or (dz == 4 and part == 0):
                out.append(("x", 1, (s, dz, 2, part)))
        elif dx == -1:
            if dz == 0:
                out.append(("x", -1, (s, dz, 2, 1)))
            elif dz in (-1, 2, -3) or (dz == 4 and part == 1):
                out.append(("x", -1, (s, dz, 2, part)))

    if mode == "z":
        if dx == 0:
            along_z()
        along_x()
    else:
        if dz == 0:
            along_x()
        if part is None or dz != 0:
            if part is None:
                along_z()
        elif part == 1:
            along_z()
    return out


def size(item):
    return SHARD * STREAMS[item[0]][3] * 2 // (1 if item[3] is None else 2)


def arrivals():
    found, items = [(s, 0, 0, None) for s in range(len(STREAMS))], []
    while found:
        for _, _, there in onward(found.pop()):
            items.append(there)
            found.append(there)
    return sorted(items, key=str)


SLOT = {item: k for k, item in enumerate(arrivals())}


class Clock:
    def __init__(self):
        self.now = 0.0
        self.free = {}
        self.due = {}
        self.coming = []
        for s, begin in enumerate(BEGIN):
            item = (s, 0, 0, None)
            heapq.heappush(self.coming, (begin, str(item), item))

    def send(self, link, count, label, rate=RATE, latency=LATENCY):
        self.now += ISSUE
        end = max(self.now, self.free.get(link, 0.0)) + count / rate
        self.free[link] = end
        self.due[label] = max(self.due.get(label, 0.0), end + latency)

    def expect(self, item):
        heapq.heappush(self.coming, (self.due[item] + MARGIN, str(item), item))


PIECES = {
    0: ((0, 0, 128),),
    1: ((0, 128, 32), (1, 0, 96)),
    2: ((1, 96, 64), (2, 0, 64)),
    3: ((2, 64, 96), (3, 0, 32)),
    4: ((3, 32, 128),),
}
ITEMS = ((0, 0),) + tuple((h, i) for i in range(8) for h in range(2) if (h, i) != (0, 0))


def kernel(
    q_hbm, k_hbm, v_hbm, docs_hbm, sink_ref, w_hbm, res_hbm, gain_hbm, up_hbm, down_hbm,
    out_hbm,
    up_all, down_all, w_ref, res_ref, q_ref, k_ref, v_ref, docs_ref, gain_ref, up_ref, down_ref,
    k_band, v_band, k_prev, v_prev, docs_prev, docs_band,
    attended, heads, mixed, normed, hidden, parts, first_a, first_b, last_a, last_b, out_ref,
    arrive, send_sems, twin_sem, twin_arrive, load_sem, halo_sem, halo_send,
    swap_sem, swap_send, row_sem, row_send, sum_sem, sum_send, end_sem, out_sem,
):
    sp = lax.axis_index("sp")
    y = lax.axis_index("tp")
    c = lax.rem(sp, 2)
    x = lax.rem(sp // 2, NX)
    z = sp // (2 * NX)

    def place(zz, xx, cc):
        return (zz * NX + xx) * 2 + cc

    def near(axis, way):
        if axis == "z":
            return {"sp": place(lax.rem(z + way + NZ, NZ), x, c), "tp": y}
        return {"sp": place(z, lax.rem(x + way + NX, NX), c), "tp": y}

    twin = {"sp": place(z, x, 1 - c), "tp": y}

    def column(by):
        return {"sp": sp, "tp": lax.rem(y + by + NY, NY)}

    def line(by):
        return {"sp": lax.rem(sp + by + 2 * NX * NZ, 2 * NX * NZ), "tp": y}

    up_load, down_load, k_load, v_load, docs_load, q_load, gain_load, res_load, w_load = loads = [
        pltpu.make_async_copy(src, dst, load_sem.at[n])
        for n, (src, dst) in enumerate((
            (up_hbm, up_ref), (down_hbm, down_ref), (k_hbm, k_ref), (v_hbm, v_ref), (docs_hbm, docs_ref),
            (q_hbm, q_ref), (gain_hbm, gain_ref), (res_hbm, res_ref), (w_hbm, w_ref),
        ))
    ]
    for load in loads:
        load.start()

    barrier = pltpu.get_barrier_semaphore()
    greeted = [near("z", 1), near("z", -1), near("x", 1), near("x", -1), twin,
               column(1), column(2), column(3), line(1), line(-1)]
    for device in greeted:
        pl.semaphore_signal(barrier, inc=1, device_id=device, device_id_type=MESH)
    pl.semaphore_wait(barrier, len(greeted))

    def remote(src, dst, send, recv, device):
        return pltpu.make_async_remote_copy(
            src_ref=src, dst_ref=dst, send_sem=send, recv_sem=recv, device_id=device, device_id_type=MESH
        )

    whole = (up_all, down_all)
    shards = (up_ref, down_ref)

    def view(item):
        s, dz, dx, part = item
        b, _, first, count = STREAMS[s]
        zz = lax.rem(z - dz + 2 * NZ, NZ)
        xx = lax.rem(x - dx + 2 * NX, NX)
        row = place(zz, xx, c) * SHARD
        rows = SHARD
        if part is not None:
            rows = SHARD // 2
            row = row + part * rows
        return whole[b].at[pl.ds(pl.multiple_of(row, 16), rows), pl.ds(first, count)]

    def own_view(s, part):
        b, _, first, count = STREAMS[s]
        if part is None:
            return shards[b].at[:, pl.ds(first, count)]
        return shards[b].at[pl.ds(part * (SHARD // 2), SHARD // 2), pl.ds(first, count)]

    clock = Clock()
    halves = set()
    left = {(b, dz): NX * SHARD * D * 2 for b in range(2) for dz in DZ_ORDER}

    def pass_on(item):
        s, dz, dx, part = item
        b = STREAMS[s][0]
        own = dz == 0 and dx == 0
        sent = onward(item)
        if STREAMS[s][1] == "x" and dz == 0 and dx == 2:
            halves.add(item)
            sent = onward((s, 0, 2, 1)) if {(s, 0, 2, 0), (s, 0, 2, 1)} <= halves else []
        for axis, way, there in sent:
            here = (s, dz, dx, there[3])
            src = own_view(s, there[3]) if own else view(here)
            remote(src, view(here), send_sems.at[b], arrive.at[SLOT[there]], near(axis, way)).start()
            clock.send((axis, way), size(there), there)
            clock.expect(there)
        src = own_view(s, part) if own else view(item)
        remote(src, view(item), twin_sem.at[b], twin_arrive.at[b, DZ_ORDER.index(dz)], twin).start()
        clock.send("twin", size(item), ("twin", b, dz), TWIN_RATE, TWIN_LATENCY)
        left[b, dz] -= size(item)

    def take():
        moment, _, item = heapq.heappop(clock.coming)
        clock.now = max(clock.now, moment)
        if item[1] != 0 or item[2] != 0:
            ref = view(item)
            remote(ref, ref, send_sems.at[0], arrive.at[SLOT[item]], twin).wait_recv()
        pass_on(item)

    def work(us):
        clock.now += us
        while clock.coming and clock.coming[0][0] <= clock.now:
            take()

    def hold(label):
        while clock.coming and clock.coming[0][0] < clock.due[label]:
            take()
        clock.now = max(clock.now, clock.due[label])

    def weights(b, dz):
        while left[b, dz] > 0:
            take()
        hold(("twin", b, dz))
        ref = whole[b].at[pl.ds(0, NX * SHARD), :]
        remote(ref, ref, twin_sem.at[b], twin_arrive.at[b, DZ_ORDER.index(dz)], twin).wait_recv()

    up_load.wait()
    work(0.0)
    for load in (k_load, v_load, docs_load):
        load.wait()

    last = pl.ds(TOK - REACH, REACH)
    docs_band[:, REACH:] = docs_ref[...].reshape(1, TOK).astype(jnp.float32)
    halo = [
        remote(k_ref.at[:, last], k_prev, halo_send.at[0], halo_sem.at[0], line(1)),
        remote(v_ref.at[:, last], v_prev, halo_send.at[1], halo_sem.at[1], line(1)),
        remote(docs_ref.at[last], docs_prev, halo_send.at[2], halo_sem.at[2], line(1)),
    ]
    for copy in halo:
        copy.start()
    clock.send("halo", 2 * HEAD * REACH * 2, "halo", RATE, 2 * LATENCY)

    own_row = pl.multiple_of(place(z, x, c) * SHARD, SHARD)
    up_all[pl.ds(own_row, SHARD), :] = up_ref[...]

    k_band[:, REACH:] = k_ref[...]
    v_band[:, REACH:] = v_ref[...]
    down_load.wait()
    down_all[pl.ds(own_row, SHARD), :] = down_ref[...]
    q_load.wait()
    ahead = (
        REACH
        + lax.broadcasted_iota(jnp.int32, (REACH, 2 * REACH), 0)
        - lax.broadcasted_iota(jnp.int32, (REACH, 2 * REACH), 1)
    )
    in_reach = (ahead >= 0) & (ahead < REACH)

    def attend(block):
        rows = pl.ds(block * REACH, REACH)
        band = pl.ds(block * REACH, 2 * REACH)
        keys = k_band[:, band]
        values = v_band[:, band]
        own_docs = docs_band[:, pl.ds((block + 1) * REACH, REACH)]
        own_docs = jnp.transpose(jnp.broadcast_to(own_docs, (REACH, REACH)))
        own_docs = jnp.concatenate([own_docs, own_docs], axis=1)
        visible = in_reach & (own_docs == docs_band[:, band])
        outs = []
        for h in range(4):
            scores = jnp.dot(
                q_ref[rows, pl.ds(h * HEAD, HEAD)], keys, preferred_element_type=jnp.float32
            ) * HEAD ** (-0.5)
            scores = jnp.where(visible, scores, masked_score)
            sink = sink_ref[h]
            top = jnp.maximum(jnp.max(scores, axis=-1, keepdims=True), sink)
            exponent = jnp.where(visible, jnp.exp(scores - top), 0.0)
            total = jnp.exp(sink - top) + jnp.sum(exponent, axis=-1, keepdims=True)
            shares = (exponent / total).astype(jnp.bfloat16)
            outs.append(
                lax.dot_general(
                    shares, values, (((1,), (1,)), ((), ())), preferred_element_type=jnp.float32
                )
            )
        attended[rows, :] = jnp.concatenate(outs, axis=1).astype(jnp.bfloat16)

    def lanes(of):
        return pl.ds(pl.multiple_of(of * 256, 256), 256)

    def hand_over(block):
        for owner, first, rows in PIECES[block]:
            @pl.when(y != owner)
            def _():
                remote(
                    attended.at[pl.ds(owner * OWN + first, rows), :], heads.at[pl.ds(first, rows), lanes(y)],
                    swap_send.at[0], swap_sem.at[y], {"sp": sp, "tp": owner},
                ).start()

    for block in (1, 2, 3):
        attend(block)
        hand_over(block)
        work(0.88)
    hold("halo")
    for copy in halo:
        copy.wait_recv()
    k_band[:, :REACH] = k_prev[...]
    v_band[:, :REACH] = v_prev[...]
    docs_band[:, :REACH] = jnp.where(sp == 0, -1.0, docs_prev[...].reshape(1, REACH).astype(jnp.float32))
    attend(0)
    hand_over(0)
    work(0.88)
    attend(4)
    hand_over(4)
    for by in (1, 3, 2):
        clock.send(("y", 1 if by < 3 else -1), OWN * 256 * 2, ("swap", by))
    heads[:, lanes(y)] = attended[pl.ds(pl.multiple_of(y * OWN, 32), OWN), :]
    work(0.1)
    w_load.wait()
    res_load.wait()
    gain_load.wait()
    for by in (1, 3, 2):
        other = lax.rem(y + by, NY)
        slot = heads.at[:, lanes(other)]
        hold(("swap", by))
        remote(slot, slot, swap_send.at[0], swap_sem.at[other], column(by)).wait_recv()

    def project(n, carry):
        cols = pl.ds(pl.multiple_of(n * 512, 512), 512)
        product = jnp.dot(heads[...], w_ref[:, cols], preferred_element_type=jnp.float32)
        product = product.astype(jnp.bfloat16).astype(jnp.float32)
        mixed[:, cols] = (res_ref[:, cols].astype(jnp.float32) + product).astype(jnp.bfloat16)
        return carry

    for half in range(2):
        lax.fori_loop(2 * half, 2 * half + 2, project, 0)
        work(0.75)

    def norm(h):
        def step(i, carry):
            rows = pl.ds(pl.multiple_of(h * HALF + i * 16, 16), 16)
            widened = mixed[rows, :].astype(jnp.float32)
            scale = lax.rsqrt(jnp.mean(widened * widened, axis=-1, keepdims=True) + epsilon)
            normed[pl.ds(pl.multiple_of((h * NY + y) * HALF + i * 16, 16), 16), :] = (
                widened * scale * gain_ref[...]
            ).astype(jnp.bfloat16)
            return carry

        lax.fori_loop(0, 5, step, 0)

    before, after, across = lax.rem(y + 3, NY), lax.rem(y + 1, NY), lax.rem(y + 2, NY)

    def row_copy(h, of, side, by, slot):
        ref = normed.at[pl.ds(pl.multiple_of((h * NY + of) * HALF, 16), HALF), pl.ds(side * (D // 2), D // 2)]
        return remote(ref, ref, row_send.at[0], row_sem.at[h, slot], column(by))

    def rows_sent(h, of, side, by, slot):
        row_copy(h, of, side, by, slot).start()
        clock.send(("y", by), HALF * D, ("row", h, slot))

    def rows_come(h, of, side, by, slot):
        hold(("row", h, slot))
        row_copy(h, of, side, by, slot).wait_recv()

    def rows_out(h):
        rows_sent(h, y, 0, 1, 0)
        rows_sent(h, y, 1, -1, 3)
        rows_sent(h, y, 1, 1, 1)
        rows_sent(h, y, 0, -1, 2)

    def rows_on(h):
        rows_come(h, before, 0, 1, 0)
        rows_sent(h, before, 0, 1, 4)
        rows_come(h, after, 1, -1, 3)
        rows_sent(h, after, 1, -1, 5)

    def rows_in(h):
        rows_come(h, before, 1, 1, 1)
        rows_come(h, after, 0, -1, 2)
        rows_come(h, across, 0, 1, 4)
        rows_come(h, across, 1, -1, 5)

    norm(0)
    rows_out(0)
    norm(1)
    work(0.4)
    rows_on(0)
    rows_out(1)
    rows_in(0)
    rows_on(1)
    for dz in DZ_ORDER:
        weights(0, dz)

    def expand(h, begin, end):
        rows = pl.ds(h * NY * HALF, NY * HALF)

        def step(n):
            cols = pl.ds(n * 512, 512)
            before_act = jnp.dot(normed[rows, :], up_all[:, cols], preferred_element_type=jnp.float32)
            hidden[rows, cols] = jnp.square(jnp.maximum(before_act, 0.0)).astype(jnp.bfloat16)

        for n in range(begin, end):
            step(n)
            work(0.8)

    def owner_rows(of):
        return pl.ds(pl.multiple_of(of * HALF, 16), HALF)

    side_a, side_b = pl.ds(0, 128), pl.ds(128, 128)
    there = set()

    def contract(h, i):
        dz = DZ_ORDER[i]
        k = h * 8 + i
        if dz not in there:
            weights(1, dz)
            there.add(dz)
        zz = lax.rem(z - dz + 2 * NZ, NZ)
        parts[k] = lax.dot_general(
            hidden[pl.ds(h * NY * HALF, NY * HALF), :], down_all[pl.ds(pl.multiple_of(zz * 256, 256), 256), :],
            (((1,), (1,)), ((), ())), preferred_element_type=jnp.float32,
        ).astype(jnp.bfloat16)
        remote(parts.at[k, owner_rows(across), side_a], first_a.at[k], sum_send.at[0], sum_sem.at[k, 0],
               column(1)).start()
        remote(parts.at[k, owner_rows(across), side_b], first_b.at[k], sum_send.at[0], sum_sem.at[k, 1],
               column(-1)).start()
        work(0.45)
        clock.send(("y", 1), HALF * 256, ("sum", k, 0))
        clock.send(("y", -1), HALF * 256, ("sum", k, 1))

    def add_and_send(h, i):
        k = h * 8 + i
        for way, (first, final, side, to, by) in enumerate((
            (first_a, last_a, side_a, after, 1), (first_b, last_b, side_b, before, -1),
        )):
            ref = first.at[k]
            hold(("sum", k, way))
            remote(ref, ref, sum_send.at[0], sum_sem.at[k, way], column(by)).wait_recv()
            rows = owner_rows(to)
            parts[k, rows, side] = (
                parts[k, rows, side].astype(jnp.float32) + first[k].astype(jnp.float32)
            ).astype(jnp.bfloat16)
            remote(parts.at[k, rows, :], final.at[k], sum_send.at[0], end_sem.at[k, way], column(by)).start()
            clock.now += 0.03
            clock.send(("y", by), HALF * 512, ("end", k, way))

    def finish(h, i):
        k = h * 8 + i
        zz = lax.rem(z - DZ_ORDER[i] + 2 * NZ, NZ)
        for way, final in enumerate((last_a, last_b)):
            ref = final.at[k]
            hold(("end", k, way))
            remote(ref, ref, sum_send.at[0], end_sem.at[k, way], column(1)).wait_recv()
        branch = (
            parts[k, owner_rows(y), :].astype(jnp.float32)
            + last_a[k].astype(jnp.float32)
            + last_b[k].astype(jnp.float32)
        )
        branch = branch.astype(jnp.bfloat16).astype(jnp.float32)
        rows = pl.ds(h * HALF, HALF)
        out_ref[rows, lanes(zz)] = (mixed[rows, lanes(zz)].astype(jnp.float32) + branch).astype(jnp.bfloat16)
        pltpu.make_async_copy(out_ref.at[rows, lanes(zz)], out_hbm.at[rows, lanes(zz)], out_sem.at[0]).start()

    expand(0, 0, 4)
    contract(*ITEMS[0])
    rows_in(1)
    expand(1, 0, 4)
    for n in range(1, len(ITEMS)):
        contract(*ITEMS[n])
        if n >= LAG:
            add_and_send(*ITEMS[n - LAG])
    for n in range(len(ITEMS) - LAG, len(ITEMS)):
        add_and_send(*ITEMS[n])
    for item in ITEMS:
        finish(*item)
    assert not clock.coming

    for b in range(2):
        ref = whole[b].at[pl.ds(0, 31 * SHARD), :]
        remote(ref, ref, send_sems.at[b], arrive.at[0], twin).wait_send()
        ref = whole[b].at[pl.ds(0, 32 * SHARD), :]
        remote(ref, ref, twin_sem.at[b], arrive.at[0], twin).wait_send()
    for copy in halo:
        copy.wait_send()
    ref = attended.at[pl.ds(0, 3 * OWN), :]
    remote(ref, ref, swap_send.at[0], arrive.at[0], twin).wait_send()
    ref = normed.at[pl.ds(0, 3 * OWN), :]
    remote(ref, ref, row_send.at[0], arrive.at[0], twin).wait_send()
    ref = parts.at[:, pl.ds(0, 3 * HALF), :]
    remote(ref, ref, sum_send.at[0], arrive.at[0], twin).wait_send()
    pltpu.make_async_copy(out_ref, out_hbm, out_sem.at[0]).wait()


def body(
    queries, keys, values, documents, sinks, out_weight, residual, norm_gain, up_weight, down_weight
):
    anywhere = pl.BlockSpec(memory_space=pl.ANY)
    bf16 = jnp.bfloat16
    dma = pltpu.SemaphoreType.DMA
    blocks = len(DZ_ORDER)
    return pl.pallas_call(
        kernel,
        out_shape=jax.ShapeDtypeStruct((OWN, D), bf16),
        in_specs=[anywhere] * 4 + [pl.BlockSpec(memory_space=pltpu.SMEM)] + [anywhere] * 5,
        out_specs=anywhere,
        scratch_shapes=[
            pltpu.VMEM((D, D), bf16),
            pltpu.VMEM((D, D), bf16),
            pltpu.VMEM((1024, D), bf16),
            pltpu.VMEM((OWN, D), bf16),
            pltpu.VMEM((TOK, 256), bf16),
            pltpu.VMEM((HEAD, TOK), bf16),
            pltpu.VMEM((HEAD, TOK), bf16),
            pltpu.VMEM((TOK,), jnp.int32),
            pltpu.VMEM((1, D), jnp.float32),
            pltpu.VMEM((SHARD, D), bf16),
            pltpu.VMEM((SHARD, D), bf16),
            pltpu.VMEM((HEAD, TOK + REACH), bf16),
            pltpu.VMEM((HEAD, TOK + REACH), bf16),
            pltpu.VMEM((HEAD, REACH), bf16),
            pltpu.VMEM((HEAD, REACH), bf16),
            pltpu.VMEM((REACH,), jnp.int32),
            pltpu.VMEM((1, TOK + REACH), jnp.float32),
            pltpu.VMEM((TOK, 256), bf16),
            pltpu.VMEM((OWN, 1024), bf16),
            pltpu.VMEM((OWN, D), bf16),
            pltpu.VMEM((TOK, D), bf16),
            pltpu.VMEM((TOK, D), bf16),
            pltpu.VMEM((2 * blocks, NY * HALF, 256), bf16),
            pltpu.VMEM((2 * blocks, HALF, 128), bf16),
            pltpu.VMEM((2 * blocks, HALF, 128), bf16),
            pltpu.VMEM((2 * blocks, HALF, 256), bf16),
            pltpu.VMEM((2 * blocks, HALF, 256), bf16),
            pltpu.VMEM((OWN, D), bf16),
            dma((len(SLOT),)),
            dma((2,)),
            dma((2,)),
            dma((2, blocks)),
            dma((9,)),
            dma((3,)),
            dma((3,)),
            dma((NY,)),
            dma((1,)),
            dma((2, 6)),
            dma((1,)),
            dma((2 * blocks, 2)),
            dma((1,)),
            dma((2 * blocks, 2)),
            dma((1,)),
        ],
        compiler_params=pltpu.CompilerParams(
            collective_id=0, has_side_effects=True, vmem_limit_bytes=60 * 1024 * 1024
        ),
    )(
        queries, keys.T, values.T, documents, sinks, out_weight, residual,
        norm_gain.reshape(1, D), up_weight, down_weight.T,
    )


def solution(mesh):
    in_specs = (
        P("sp", "tp"),
        P("sp", "tp"),
        P("sp", "tp"),
        P("sp"),
        P("tp"),
        P(),
        P(("sp", "tp"), None),
        P(),
        P("sp", "tp"),
        P("tp", "sp"),
    )
    out_specs = P(("sp", "tp"), None)
    return jax.shard_map(body, mesh=mesh, in_specs=in_specs, out_specs=out_specs, check_vma=False)
```

time: 95.6 us -> 82.3 us (0.86)
  Pallas kernels: 92 us -> 80.2 us
  local copies, waits for them, and re-layouts: 3.25 us -> 1.98 us
    pallas_call x1, Pallas kernels: 92 us -> 80.2 us  [body(): pl.pallas_call(kernel, out_shape=jax.ShapeDtypeStruct((OWN, D), bf16), in...]
    reshape x1 -> x0, local copies, waits for them, and re-layouts: 1.27 us -> none  [body(): documents.reshape(1, TOK)]
where the time goes in v2:
time: 82.3 us; the launch traced here: 82.2 us
  Pallas kernels  80.2 us (97%)
  local copies, waits for them, and re-layouts  1.98 us (2%)
    pallas_call x1, Pallas kernels, body(): pl.pallas_call(kernel, out_shape=jax.ShapeDtypeStruct((OWN, D), bf16), in...  80.2 us
    unnamed x1, local copies, waits for them, and re-layouts  1.98 us

profile of v2, /device:TPU:1, one launch (start us, length us, event | category | flops | bytes accessed | tf_op | source)
XLA Modules:
  0.0 82.2 jit_solution(13409149653712957469)
XLA Ops:
  0.0 80.2 %shard_map.100 = bf16[160,2048]{1,0:T(8,128)(2,1)} custom-call(bf16[640,256]{1,0:T(8,128)(2,1)} %q_hbm.1, bf16[64,640]{1,0:T(8,128)(2,1)} %bitcast.5, bf16[64,640]{1,0:T(8,128)(2,1)} %bitcast.6, s32[640]{0:T(1024)} %docs_hbm.1, f32[4]{0:T(128)} %sink_ref.1, bf16[1024,2048]{1,0:T(8,128)(2,1)} %w_hbm.1, bf16[160,2048]{1,0:T(8,128)(2,1)} %res_hbm.1, ...), custom_call_target="tpu_custom_call" | custom-call | tf_op jit(solution)/shard_map/pallas_call | solution.py:523
  80.2 2.0 %copy.12 = bf16[160,2048]{1,0:T(8,128)(2,1)} copy(bf16[160,2048]{1,0:T(8,128)(2,1)} %shard_map.100) | data formatting | bytes 1310720

commit v3 on v2

--- a/solution.py
+++ b/solution.py
@@ -21,8 +21,8 @@
 epsilon = 1e-06
 
 CUT = 1280
-STREAMS = ((0, "z", 0, CUT), (0, "x", CUT, D - CUT), (1, "z", 0, CUT), (1, "x", CUT, D - CUT))
-BEGIN = (0.0, 0.0, 20.0, 20.0)
+STREAMS = ((0, "z", 0, CUT), (0, "x", CUT, D - CUT), (1, "z", 0, 1152), (1, "x", 1152, D - 1152))
+BEGIN = (0.0, 0.0, 20.0, 17.0)
 RATE = 46.6e3
 LATENCY = 1.8
 TWIN_RATE = 600e3

time: 82.3 us -> 81.5 us (level)
  no operation moved by 1% of the time
where the time goes in v3:
time: 81.5 us; the launch traced here: 81.4 us
  Pallas kernels  79.4 us (97%)
  local copies, waits for them, and re-layouts  1.98 us (2%)
    pallas_call x1, Pallas kernels, body(): pl.pallas_call(kernel, out_shape=jax.ShapeDtypeStruct((OWN, D), bf16), in...  79.4 us
    unnamed x1, local copies, waits for them, and re-layouts  1.98 us

profile of v3, /device:TPU:1, one launch (start us, length us, event | category | flops | bytes accessed | tf_op | source)
XLA Modules:
  0.0 81.4 jit_solution(4063519528848406396)
XLA Ops:
  0.0 79.4 %shard_map.100 = bf16[160,2048]{1,0:T(8,128)(2,1)} custom-call(bf16[640,256]{1,0:T(8,128)(2,1)} %q_hbm.1, bf16[64,640]{1,0:T(8,128)(2,1)} %bitcast.5, bf16[64,640]{1,0:T(8,128)(2,1)} %bitcast.6, s32[640]{0:T(1024)} %docs_hbm.1, f32[4]{0:T(128)} %sink_ref.1, bf16[1024,2048]{1,0:T(8,128)(2,1)} %w_hbm.1, bf16[160,2048]{1,0:T(8,128)(2,1)} %res_hbm.1, ...), custom_call_target="tpu_custom_call" | custom-call | tf_op jit(solution)/shard_map/pallas_call | solution.py:523
  79.4 2.0 %copy.12 = bf16[160,2048]{1,0:T(8,128)(2,1)} copy(bf16[160,2048]{1,0:T(8,128)(2,1)} %shard_map.100) | data formatting | bytes 1310720

commit v4 on v3

--- a/solution.py
+++ b/solution.py
@@ -22,7 +22,7 @@
 
 CUT = 1280
 STREAMS = ((0, "z", 0, CUT), (0, "x", CUT, D - CUT), (1, "z", 0, 1152), (1, "x", 1152, D - 1152))
-BEGIN = (0.0, 0.0, 20.0, 17.0)
+BEGIN = (0.0, 0.0, 20.0, 16.0)
 RATE = 46.6e3
 LATENCY = 1.8
 TWIN_RATE = 600e3

time: 81.5 us -> 85.6 us (1.050)
  Pallas kernels: 79.4 us -> 83.5 us
    pallas_call x1, Pallas kernels: 79.4 us -> 83.5 us  [body(): pl.pallas_call(kernel, out_shape=jax.ShapeDtypeStruct((OWN, D), bf16), in...]
where the time goes in v4:
time: 85.6 us; the launch traced here: 85.5 us
  Pallas kernels  83.5 us (98%)
  local copies, waits for them, and re-layouts  1.98 us (2%)
    pallas_call x1, Pallas kernels, body(): pl.pallas_call(kernel, out_shape=jax.ShapeDtypeStruct((OWN, D), bf16), in...  83.5 us
    unnamed x1, local copies, waits for them, and re-layouts  1.98 us

profile of v4, /device:TPU:1, one launch (start us, length us, event | category | flops | bytes accessed | tf_op | source)
XLA Modules:
  0.0 85.5 jit_solution(14419026249391271660)
XLA Ops:
  0.0 83.5 %shard_map.100 = bf16[160,2048]{1,0:T(8,128)(2,1)} custom-call(bf16[640,256]{1,0:T(8,128)(2,1)} %q_hbm.1, bf16[64,640]{1,0:T(8,128)(2,1)} %bitcast.5, bf16[64,640]{1,0:T(8,128)(2,1)} %bitcast.6, s32[640]{0:T(1024)} %docs_hbm.1, f32[4]{0:T(128)} %sink_ref.1, bf16[1024,2048]{1,0:T(8,128)(2,1)} %w_hbm.1, bf16[160,2048]{1,0:T(8,128)(2,1)} %res_hbm.1, ...), custom_call_target="tpu_custom_call" | custom-call | tf_op jit(solution)/shard_map/pallas_call | solution.py:523
  83.5 2.0 %copy.12 = bf16[160,2048]{1,0:T(8,128)(2,1)} copy(bf16[160,2048]{1,0:T(8,128)(2,1)} %shard_map.100) | data formatting | bytes 1310720
